TPU v7x, 32 devices: a whole 2x2x4 slice. The times are simulated.
32 devices in a mesh: kv: 4 (over y, x), tp: 8 (over z, core).
Axes of the slice: x: 2, y: 2, z: 4, core: 2. Of those that a mesh axis runs over, the one named last changes fastest.
Arguments:
- stream: bfloat16 [32, 4096], P(None, ('kv', 'tp')), may hold values from -18 to 18
- mixer_gain: float32 [4096], replicated, may hold values from 0.1 to 1.9
- query_weight: bfloat16 [4096, 1024], P(None, 'tp'), may hold values from -0.09375 to 0.09375
- key_weight: bfloat16 [4096, 1024], P(None, 'tp'), may hold values from -0.09375 to 0.09375
- value_weight: bfloat16 [4096, 1024], P(None, 'tp'), may hold values from -0.09375 to 0.09375
- forget_weight: bfloat16 [4096, 16], replicated, may hold values from -0.09375 to 0.09375
- forget_bias: float32 [16], replicated, may hold values from -4 to -2
- key_cache: bfloat16 [32, 16, 4096, 64], P(None, 'tp', 'kv'), may hold values from -512 to 512, as said below
- value_cache: bfloat16 [32, 16, 4096, 64], P(None, 'tp', 'kv'), may hold values from -12 to 12
- past_decay: float32 [32, 16, 4096], P(None, 'tp', 'kv'), may hold values from -4096 to 0, as said below
- out_weight: bfloat16 [1024, 4096], P('tp', 'kv'), may hold values from -0.75 to 0.75
- channel_gain: float32 [4096], replicated, may hold values from 0.1 to 1.9
- up_weight: bfloat16 [4096, 16384], P('kv', 'tp'), may hold values from -0.09375 to 0.09375
- down_weight: bfloat16 [16384, 4096], P('tp', 'kv'), may hold values from -0.0625 to 0.0625
Outputs:
- updated: bfloat16 [32, 4096], P(None, ('kv', 'tp'))
Inputs may be any that keep to these rules, and one draw needn't show every extreme that they name: `key_cache`: keys of order one; some cached keys may be much larger. `past_decay`: never falling along the positions of a sequence and head, zero at the last cached position.
All inputs are finite; a program needn't handle non-finite values.
Results may differ from a plain program's by a relative error of at most 0.014.
The roundings to bfloat16 on the way count: a program that leaves them out, or rounds other values in their place, can miss the bound.
Values may be sent and summed in bfloat16 or wider, within the bound.
No kernel may reach another device: no remote copies, remote signals or barrier semaphores. Data moves between devices by JAX's collectives and lax.ppermute only.
A program may use at most 64 MiB of HBM per device.

v0:
```python
import jax
import jax.numpy as jnp
from jax import lax
from jax.sharding import PartitionSpec as P

D = 4096
EPS = 1e-06


def combined_all(part, axis, combine):
    gathered = jax.tree.map(lambda a: lax.all_gather(a, axis), part)

    def take(source):
        return jax.tree.map(lambda a: lax.dynamic_index_in_dim(a, source, 0, False), gathered)

    return lax.fori_loop(
        1, lax.axis_size(axis), lambda source, state: combine(state, take(source)), take(0)
    )


def rms_scale(values, gain):
    widened = values.astype(jnp.float32)
    inverse = lax.rsqrt(jnp.mean(widened * widened, axis=-1, keepdims=True) + EPS)
    return (widened * inverse * gain).astype(jnp.bfloat16)


def merge_parts(earlier, later):
    top_one, total_one, sums_one = earlier
    top_two, total_two, sums_two = later
    highest = jnp.maximum(top_one, top_two)
    factor_one = jnp.exp(top_one - highest)
    factor_two = jnp.exp(top_two - highest)
    return (
        highest,
        total_one * factor_one + total_two * factor_two,
        sums_one * factor_one[..., None] + sums_two * factor_two[..., None],
    )


def squared_relu(values):
    return jnp.square(jax.nn.relu(values)).astype(jnp.bfloat16)


def row_squares(values):
    widened = values.astype(jnp.float32)
    return jnp.sum(widened * widened, axis=1)


def shards(
    stream,
    mixer_gain,
    query_weight,
    key_weight,
    value_weight,
    forget_weight,
    forget_bias,
    key_cache,
    value_cache,
    past_decay,
    out_weight,
    channel_gain,
    up_weight,
    down_weight,
):
    batch_rows = stream.shape[0]
    local_heads = key_cache.shape[1]
    head_size = key_cache.shape[3]
    scale_factor = float(head_size) ** (-0.5)
    gathered = lax.all_gather(stream, ("kv", "tp"), axis=1, tiled=True)
    normed = rms_scale(gathered, mixer_gain)
    queries = jnp.dot(normed, query_weight, preferred_element_type=jnp.float32).astype(jnp.bfloat16)
    keys_new = jnp.dot(normed, key_weight, preferred_element_type=jnp.float32).astype(jnp.bfloat16)
    values_new = jnp.dot(normed, value_weight, preferred_element_type=jnp.float32).astype(
        jnp.bfloat16
    )
    forget_all = jax.nn.log_sigmoid(
        jnp.dot(normed, forget_weight, preferred_element_type=jnp.float32) + forget_bias
    )
    forget = lax.dynamic_slice_in_dim(
        forget_all, lax.axis_index("tp") * local_heads, local_heads, 1
    )
    query_heads = queries.reshape(batch_rows, local_heads, head_size)
    scores = (
        jnp.einsum("bhd,bhpd->bhp", query_heads, key_cache, preferred_element_type=jnp.float32)
        * scale_factor
        + forget[..., None]
        + past_decay
    )
    highest = jnp.max(scores, axis=-1)
    weights = jnp.exp(scores - highest[..., None]).astype(jnp.bfloat16)
    totals = jnp.sum(weights.astype(jnp.float32), axis=-1)
    sums = jnp.einsum("bhp,bhpd->bhd", weights, value_cache, preferred_element_type=jnp.float32)
    highest, totals, sums = combined_all((highest, totals, sums), "kv", merge_parts)
    key_heads = keys_new.reshape(batch_rows, local_heads, head_size).astype(jnp.float32)
    value_heads = values_new.reshape(batch_rows, local_heads, head_size).astype(jnp.float32)
    own = jnp.sum(query_heads.astype(jnp.float32) * key_heads, axis=-1) * scale_factor
    peak = jnp.maximum(highest, own)
    cache_factor = jnp.exp(highest - peak)
    own_factor = jnp.exp(own - peak)
    numer = sums * cache_factor[..., None] + value_heads * own_factor[..., None]
    denom = totals * cache_factor + own_factor
    attention = (
        (numer / denom[..., None]).astype(jnp.bfloat16).reshape(batch_rows, local_heads * head_size)
    )
    partial_value = jnp.dot(attention, out_weight, preferred_element_type=jnp.float32)
    piece_width = stream.shape[1]
    block_width = partial_value.shape[1]
    block_sum = lax.psum(partial_value, "tp")
    own_block = lax.dynamic_slice_in_dim(
        gathered, lax.axis_index("kv") * block_width, block_width, 1
    )
    middle_block = (own_block.astype(jnp.float32) + block_sum).astype(jnp.bfloat16)
    squares = lax.psum(row_squares(middle_block), "kv")
    middle_piece = lax.dynamic_slice_in_dim(
        middle_block, lax.axis_index("tp") * piece_width, piece_width, 1
    )
    inverse = lax.rsqrt(squares / D + EPS)
    gain_block = lax.dynamic_slice_in_dim(
        channel_gain, lax.axis_index("kv") * block_width, block_width, 0
    )
    mixed_block = (
        middle_block.astype(jnp.float32) * inverse[:, None] * gain_block[None, :]
    ).astype(jnp.bfloat16)
    up_partial = jnp.dot(mixed_block, up_weight, preferred_element_type=jnp.float32)
    hidden = squared_relu(lax.psum(up_partial, "kv"))
    down_partial = jnp.dot(hidden, down_weight, preferred_element_type=jnp.float32)
    reduced = lax.psum_scatter(down_partial, "tp", scatter_dimension=1, tiled=True)
    return (middle_piece.astype(jnp.float32) + reduced).astype(jnp.bfloat16)


def solution(mesh):
    return jax.shard_map(
        shards,
        mesh=mesh,
        in_specs=(
            P(None, ("kv", "tp")),
            P(),
            P(None, "tp"),
            P(None, "tp"),
            P(None, "tp"),
            P(),
            P(),
            P(None, "tp", "kv", None),
            P(None, "tp", "kv", None),
            P(None, "tp", "kv"),
            P("tp", "kv"),
            P(),
            P("kv", "tp"),
            P("tp", "kv"),
        ),
        out_specs=P(None, ("kv", "tp")),
        check_vma=False,
    )
```

profile of v0, /device:TPU:0, one launch (start us, length us, event | category | flops | bytes accessed | tf_op | source)
XLA Modules:
  0.0 247.9 jit_solution(13276194251928122677)
XLA Ops:
  6.5 44.6 %all_gather.21 = bf16[32,4096]{1,0:T(8,128)(2,1)S(1)} all-gather(bf16[32,128]{1,0:T(8,128)(2,1)} %param.16), channel_id=1, replica_groups=mesh['kv'=4,'tp'=8] {'kv','tp'}, dimensions={1}, use_global_device_ids=true | all-gather | bytes 270336 | tf_op jit(solution)/shard_map/all_gather | solution.py:69
  51.2 0.2 fusion.6
  51.4 1.0 convolution_convert_fusion.2
  52.6 1.2 fusion.40
  53.9 4.6 %fusion.41 = f32[32,2,1,1024]{3,2,1,0:T(1,128)S(1)} fusion(bf16[32,2,64,1]{2,3,1,0:T(2,128)(2,1)S(1)} %reshape.57, bf16[32,2,1024,64]{2,3,1,0:T(8,128)(2,1)} %param.23), kind=kOutput, calls=%fused_computation.63 | convolution fusion | flops 8388608 | bytes 8658944 | tf_op jit(solution)/shard_map/bhd,bhpd->bhp/dot_general | solution.py:84
  58.5 2.1 fusion.38
  60.6 1.3 fusion.30
  61.9 5.7 %fusion.11 = f32[32,2,1,64]{3,2,1,0:T(1,128)S(1)} fusion(bf16[32,2,1024,64]{2,3,1,0:T(8,128)(2,1)} %param.24, bf16[32,2,1024,1]{2,1,0,3:T(2,128)(2,1)S(1)} %get-tuple-element.211), kind=kOutput, calls=%fused_computation.24 | convolution fusion | flops 8388608 | bytes 8536064 | tf_op jit(solution)/shard_map/bhp,bhpd->bhd/dot_general | solution.py:92
  67.6 7.5 %all-gather.2 = f32[128,2,64]{2,1,0:T(2,128)S(1)} all-gather(f32[32,2,64]{2,1,0:T(2,128)S(1)} %bitcast.49), channel_id=4, replica_groups=mesh['kv'=4,'tp'=8] {'kv'}, dimensions={0}, use_global_device_ids=true | all-gather | bytes 81920 | tf_op jit(solution)/shard_map/all_gather | solution.py:11
  75.0 0.6 copy-done.3
  75.8 8.1 %all-gather.4 = f32[4,32,2]{1,2,0:T(2,128)S(1)} all-gather(f32[1,32,2]{1,2,0:T(2,128)S(1)} %bitcast.51), channel_id=3, replica_groups=mesh['kv'=4,'tp'=8] {'kv'}, dimensions={0}, use_global_device_ids=true | all-gather | bytes 1280 | tf_op jit(solution)/shard_map/all_gather | solution.py:11
  83.8 7.1 %all-gather.3 = f32[4,32,2]{1,2,0:T(2,128)S(1)} all-gather(f32[1,32,2]{1,2,0:T(2,128)S(1)} %bitcast.50), channel_id=2, replica_groups=mesh['kv'=4,'tp'=8] {'kv'}, dimensions={0}, use_global_device_ids=true | all-gather | bytes 1280 | tf_op jit(solution)/shard_map/all_gather | solution.py:11
  90.9 3.6 %while.19 = (s32[]{:T(128)}, f32[32,2]{0,1:T(2,128)S(1)}, f32[32,2]{0,1:T(2,128)S(1)}, f32[32,2,64]{2,1,0:T(2,128)S(1)}, f32[4,32,2]{1,2,0:T(2,128)S(1)}, /*inde...) while((s32[]{:T(128)}, f32[32,2]{0,1:T(2,128)S(1)}, ...), condition=%wide.region_4.5_spmd, body=%wide.region_3.4_spmd.sunk | while | flops 12677 | bytes 52887 | solution.py:16
  91.1 1.0 fusion.57
  92.3 1.0 fusion.57
  93.5 1.0 fusion.57
  94.6 0.3 fusion.4
  94.9 0.1 reshape.33
  95.0 0.1 multiply_reduce_fusion
  95.2 0.1 copy.36
  95.5 0.3 fusion.3
  95.9 0.2 fusion.22
  96.2 1.8 fusion.42
  98.0 0.7 dynamic_slice.59
  98.7 51.7 %all-reduce.3.cloned.1.call-done = f32[32,1024]{1,0:T(8,128)} async-done(((f32[32,1024]{1,0:T(8,128)}), f32[32,1024]{1,0:T(8,128)}) %all-reduce.3.cloned.1.call-update) | async-done | bytes 131088 | tf_op jit(solution)/shard_map/psum | solution.py:108
  150.4 1.0 fusion.13
  151.4 9.8 %psum.22 = f32[32]{0:T(128)S(1)} all-reduce(f32[32]{0:T(128)S(1)} %get-tuple-element.204), channel_id=1, replica_groups=mesh['kv'=4,'tp'=8] {'kv'}, use_global_device_ids=true, to_apply=%region_8.9 | all-reduce | flops 32 | bytes 256 | tf_op jit(solution)/shard_map/psum | solution.py:113
  161.3 3.8 %fusion.18 = f32[32,2048]{1,0:T(8,128)} fusion(bf16[1024,2048]{1,0:T(8,128)(2,1)} %param.28, bf16[32,1024]{1,0:T(8,128)(2,1)S(1)} %get-tuple-element.205, f32[1024]{0:T(1024)S(1)} %dynamic_slice.59, f32[32]{0:T(128)S(1)} %add_rsqrt_fusion), kind=kOutput, calls=%fused_computation.37 | convolution fusion | flops 134348800 | bytes 4526208 | tf_op jit(solution)/shard_map/dot_general | solution.py:124
  165.1 40.4 %all-reduce.5.cloned.1.call-done = f32[32,2048]{1,0:T(8,128)} async-done(((f32[32,2048]{1,0:T(8,128)}), f32[32,2048]{1,0:T(8,128)}) %all-reduce.5.cloned.1.call-update) | async-done | bytes 262160 | tf_op jit(solution)/shard_map/psum | solution.py:125
  205.5 3.8 %fusion.16 = f32[32,1024]{1,0:T(8,128)} fusion(bf16[2048,1024]{1,0:T(8,128)(2,1)} %param.29, f32[32,2048]{1,0:T(8,128)} %all-reduce.5.cloned.1.call-done), kind=kOutput, calls=%fused_computation.34 | convolution fusion | flops 134414336 | bytes 4587520 | tf_op jit(solution)/shard_map/dot_general | solution.py:126
  209.3 30.7 %reduce-scatter.2.cloned.1.call-done = f32[32,128]{1,0:T(8,128)} async-done(((f32[32,1024]{1,0:T(8,128)}), f32[32,128]{1,0:T(8,128)}) %reduce-scatter.2.cloned.1.call-update) | async-done | bytes 16400 | tf_op jit(solution)/shard_map/reduce_scatter | solution.py:127
  240.0 1.3 add_convert_fusion.1
  (41 shorter events, 1.6 us)
Async XLA Ops:
  6.5 44.8 %copy-start = (bf16[4096,128]{1,0:T(8,128)(2,1)S(1)}, bf16[4096,128]{1,0:T(8,128)(2,1)}, u32[]{:S(2)}) copy-start(bf16[4096,128]{1,0:T(8,128)(2,1)} %param.18) | copy-start | bytes 3145732
  6.5 143.8 %all-reduce.3.cloned.1.call-start = ((), (), s32[]{:S(2)}) async-start(), calls=%async_computation.1 | async-start | bytes 262144 | tf_op jit(solution)/shard_map/psum | solution.py:108
  58.4 36.1 %copy-start.1 = (bf16[4096,128]{1,0:T(8,128)(2,1)S(1)}, bf16[4096,128]{1,0:T(8,128)(2,1)}, u32[]{:S(2)}) copy-start(bf16[4096,128]{1,0:T(8,128)(2,1)} %param.19) | copy-start | bytes 3145732
  58.4 36.1 %copy-start.4 = (f32[4096]{0:T(1024)S(1)}, f32[4096]{0:T(1024)}, u32[]{:S(2)}) copy-start(f32[4096]{0:T(1024)} %param.17) | copy-start | bytes 49156
  58.5 37.0 %copy-start.2 = (bf16[4096,128]{1,0:T(8,128)(2,1)S(1)}, bf16[4096,128]{1,0:T(8,128)(2,1)}, u32[]{:S(2)}) copy-start(bf16[4096,128]{1,0:T(8,128)(2,1)} %param.20) | copy-start | bytes 3145732
  75.0 0.6 copy-start.3
  98.0 107.5 %all-reduce.5.cloned.1.call-start = ((), (), s32[]{:S(2)}) async-start(), calls=%async_computation.2 | async-start | bytes 524288 | tf_op jit(solution)/shard_map/psum | solution.py:125
  165.1 75.0 %reduce-scatter.2.cloned.1.call-start = ((), (), s32[]{:S(2)}) async-start(), calls=%async_computation.3 | async-start | bytes 147456 | tf_op jit(solution)/shard_map/reduce_scatter | solution.py:127
Sparse Core Ops, SparseCore 0:
  98.1 52.2 all-reduce.2
  165.2 40.2 all-reduce.4
  209.4 30.5 reduce-scatter.1
where the time goes:
time: 249 us; the launch traced here: 248 us
  waiting for transfers between devices  123 us (49%)
  blocking collectives  77.1 us (31%)
  matrix products  22.4 us (9%)
  between operations  13.2 us (5%)
  other arithmetic  9.28 us (4%)
  local copies, waits for them, and re-layouts  2.9 us (1%)
    psum x1, waiting for transfers between devices, shards(): block_sum = lax.psum(partial_value, 'tp')  51.7 us
    all_gather x1, blocking collectives, shards(): gathered = lax.all_gather(stream, ('kv', 'tp'), axis=1, tiled=True)  44.6 us
    psum x1, waiting for transfers between devices, shards(): hidden = squared_relu(lax.psum(up_partial, 'kv'))  40.4 us
    reduce_scatter x1, waiting for transfers between devices, shards(): lax.psum_scatter(down_partial, 'tp', scatter_dimension=1, tiled=True)  30.7 us
    all_gather x3, blocking collectives, combined_all(): gathered = jax.tree.map(lambda a: lax.all_gather(a, axis), part)  22.6 us
    psum x1, blocking collectives, shards(): squares = lax.psum(row_squares(middle_block), 'kv')  9.84 us
    dot_general x1, matrix products, shards(): jnp.einsum('bhp,bhpd->bhd', weights, value_cache, preferred_element_type=...  5.65 us
  transfers between devices with their start and end apart: 3, of which 3 were waited for; matrix products, arithmetic and copies ran while one was open for 0% of the time, Pallas kernels for 0%

commit v1 on v0

--- a/solution.py
+++ b/solution.py
@@ -105,7 +105,10 @@
     partial_value = jnp.dot(attention, out_weight, preferred_element_type=jnp.float32)
     piece_width = stream.shape[1]
     block_width = partial_value.shape[1]
-    block_sum = lax.psum(partial_value, "tp")
+    size, block_sum = (lax.axis_size("tp"), partial_value)
+    for reach in [1 << k for k in range(size.bit_length() - 1)]:
+        swap = [(i, i ^ reach) for i in range(size)]
+        block_sum = block_sum + lax.ppermute(block_sum, "tp", swap)
     own_block = lax.dynamic_slice_in_dim(
         gathered, lax.axis_index("kv") * block_width, block_width, 1
     )

time: 249 us -> 210 us (0.84)
  waiting for transfers between devices: 123 us -> 85.7 us
    psum x1 -> x0, waiting for transfers between devices: 51.7 us -> none  [shards(): block_sum = lax.psum(partial_value, 'tp')]
    ppermute x0 -> x3, waiting for transfers between devices: none -> 14.6 us  [shards(): block_sum = block_sum + lax.ppermute(block_sum, 'tp', swap)]
  transfers between devices with their start and end apart: 3 -> 5, of which waited for: 3 -> 5; matrix products, arithmetic and copies ran while one was open for 0% -> 0% of each run, Pallas kernels for 0% -> 0%
where the time goes in v1:
time: 210 us; the launch traced here: 209 us
  waiting for transfers between devices  85.7 us (41%)
  blocking collectives  76.2 us (36%)
  matrix products  21.7 us (10%)
  between operations  13.6 us (6%)
  other arithmetic  8.41 us (4%)
  local copies, waits for them, and re-layouts  2.9 us (1%)
    all_gather x1, blocking collectives, shards(): gathered = lax.all_gather(stream, ('kv', 'tp'), axis=1, tiled=True)  44.6 us
    psum x1, waiting for transfers between devices, shards(): hidden = squared_relu(lax.psum(up_partial, 'kv'))  40.4 us
    reduce_scatter x1, waiting for transfers between devices, shards(): lax.psum_scatter(down_partial, 'tp', scatter_dimension=1, tiled=True)  30.7 us
    all_gather x3, blocking collectives, combined_all(): gathered = jax.tree.map(lambda a: lax.all_gather(a, axis), part)  22.6 us
    ppermute x3, waiting for transfers between devices, shards(): block_sum = block_sum + lax.ppermute(block_sum, 'tp', swap)  14.6 us
    psum x1, blocking collectives, shards(): squares = lax.psum(row_squares(middle_block), 'kv')  8.98 us
    dot_general x1, matrix products, shards(): jnp.einsum('bhp,bhpd->bhd', weights, value_cache, preferred_element_type=...  5.65 us
    dot_general x1, matrix products, shards(): jnp.einsum('bhd,bhpd->bhp', query_heads, key_cache, preferred_element_typ...  4.59 us
  transfers between devices with their start and end apart: 5, of which 5 were waited for; matrix products, arithmetic and copies ran while one was open for 0% of the time, Pallas kernels for 0%

profile of v1, /device:TPU:0, one launch (start us, length us, event | category | flops | bytes accessed | tf_op | source)
XLA Modules:
  0.0 208.8 jit_solution(2053224941343637644)
XLA Ops:
  6.5 44.6 %all_gather.21 = bf16[32,4096]{1,0:T(8,128)(2,1)S(1)} all-gather(bf16[32,128]{1,0:T(8,128)(2,1)} %param.16), channel_id=1, replica_groups=mesh['kv'=4,'tp'=8] {'kv','tp'}, dimensions={1}, use_global_device_ids=true | all-gather | bytes 270336 | tf_op jit(solution)/shard_map/all_gather | solution.py:69
  51.2 0.2 fusion.6
  51.4 1.0 convolution_convert_fusion.2
  52.6 1.2 fusion.40
  53.9 4.6 %fusion.41 = f32[32,2,1,1024]{3,2,1,0:T(1,128)S(1)} fusion(bf16[32,2,64,1]{2,3,1,0:T(2,128)(2,1)S(1)} %reshape.57, bf16[32,2,1024,64]{2,3,1,0:T(8,128)(2,1)} %param.23), kind=kOutput, calls=%fused_computation.63 | convolution fusion | flops 8388608 | bytes 8658944 | tf_op jit(solution)/shard_map/bhd,bhpd->bhp/dot_general | solution.py:84
  58.5 2.1 fusion.38
  60.6 1.3 fusion.30
  61.9 5.7 %fusion.11 = f32[32,2,1,64]{3,2,1,0:T(1,128)S(1)} fusion(bf16[32,2,1024,64]{2,3,1,0:T(8,128)(2,1)} %param.24, bf16[32,2,1024,1]{2,1,0,3:T(2,128)(2,1)S(1)} %get-tuple-element.211), kind=kOutput, calls=%fused_computation.24 | convolution fusion | flops 8388608 | bytes 8536064 | tf_op jit(solution)/shard_map/bhp,bhpd->bhd/dot_general | solution.py:92
  67.6 7.5 %all-gather.2 = f32[128,2,64]{2,1,0:T(2,128)S(1)} all-gather(f32[32,2,64]{2,1,0:T(2,128)S(1)} %bitcast.49), channel_id=4, replica_groups=mesh['kv'=4,'tp'=8] {'kv'}, dimensions={0}, use_global_device_ids=true | all-gather | bytes 81920 | tf_op jit(solution)/shard_map/all_gather | solution.py:11
  75.0 0.6 copy-done.3
  75.8 8.1 %all-gather.4 = f32[4,32,2]{1,2,0:T(2,128)S(1)} all-gather(f32[1,32,2]{1,2,0:T(2,128)S(1)} %bitcast.51), channel_id=3, replica_groups=mesh['kv'=4,'tp'=8] {'kv'}, dimensions={0}, use_global_device_ids=true | all-gather | bytes 1280 | tf_op jit(solution)/shard_map/all_gather | solution.py:11
  83.8 7.1 %all-gather.3 = f32[4,32,2]{1,2,0:T(2,128)S(1)} all-gather(f32[1,32,2]{1,2,0:T(2,128)S(1)} %bitcast.50), channel_id=2, replica_groups=mesh['kv'=4,'tp'=8] {'kv'}, dimensions={0}, use_global_device_ids=true | all-gather | bytes 1280 | tf_op jit(solution)/shard_map/all_gather | solution.py:11
  90.9 3.6 %while.19 = (s32[]{:T(128)}, f32[32,2]{0,1:T(2,128)S(1)}, f32[32,2]{0,1:T(2,128)S(1)}, f32[32,2,64]{2,1,0:T(2,128)S(1)}, f32[4,32,2]{1,2,0:T(2,128)S(1)}, /*inde...) while((s32[]{:T(128)}, f32[32,2]{0,1:T(2,128)S(1)}, ...), condition=%wide.region_4.5_spmd, body=%wide.region_3.4_spmd.sunk | while | flops 12677 | bytes 52887 | solution.py:16
  91.1 1.0 fusion.57
  92.3 1.0 fusion.57
  93.5 1.0 fusion.57
  94.6 0.3 fusion.4
  95.0 0.1 multiply_reduce_fusion
  95.5 0.3 fusion.3
  95.9 0.2 fusion.22
  96.2 1.1 fusion.42
  97.4 1.3 collective-permute-done
  98.8 5.5 %collective-permute-done.1 = f32[32,1024]{1,0:T(8,128)S(1)} collective-permute-done((f32[32,1024]{1,0:T(8,128)S(1)}, f32[32,1024]{1,0:T(8,128)S(1)}, u32[]{:S(2)}, u32[]{:S(2)}) %collective-permute-start.1) | collective-permute-done | bytes 131104 | tf_op jit(solution)/shard_map/ppermute | solution.py:111
  104.4 0.7 dynamic_slice.59
  105.1 7.7 %collective-permute-done.2 = f32[32,1024]{1,0:T(8,128)S(1)} collective-permute-done((f32[32,1024]{1,0:T(8,128)S(1)}, f32[32,1024]{1,0:T(8,128)S(1)}, u32[]{:S(2)}, u32[]{:S(2)}) %collective-permute-start.2) | collective-permute-done | bytes 131104 | tf_op jit(solution)/shard_map/ppermute | solution.py:111
  112.8 0.1 fusion.13
  113.0 9.0 %psum.14 = f32[32]{0:T(128)S(1)} all-reduce(f32[32]{0:T(128)S(1)} %get-tuple-element.204), channel_id=1, replica_groups=mesh['kv'=4,'tp'=8] {'kv'}, use_global_device_ids=true, to_apply=%region_7.8 | all-reduce | flops 32 | bytes 256 | tf_op jit(solution)/shard_map/psum | solution.py:116
  121.9 3.8 %fusion.18 = f32[32,2048]{1,0:T(8,128)} fusion(bf16[1024,2048]{1,0:T(8,128)(2,1)} %param.28, bf16[32,1024]{1,0:T(8,128)(2,1)S(1)} %get-tuple-element.205, f32[1024]{0:T(1024)S(1)} %dynamic_slice.59, f32[32]{0:T(128)S(1)} %add_rsqrt_fusion), kind=kOutput, calls=%fused_computation.37 | convolution fusion | flops 134348800 | bytes 4526208 | tf_op jit(solution)/shard_map/dot_general | solution.py:127
  125.8 40.4 %all-reduce.2.cloned.1.call-done = f32[32,2048]{1,0:T(8,128)} async-done(((f32[32,2048]{1,0:T(8,128)}), f32[32,2048]{1,0:T(8,128)}) %all-reduce.2.cloned.1.call-update) | async-done | bytes 262160 | tf_op jit(solution)/shard_map/psum | solution.py:128
  166.1 3.8 %fusion.16 = f32[32,1024]{1,0:T(8,128)} fusion(bf16[2048,1024]{1,0:T(8,128)(2,1)} %param.29, f32[32,2048]{1,0:T(8,128)} %all-reduce.2.cloned.1.call-done), kind=kOutput, calls=%fused_computation.34 | convolution fusion | flops 134414336 | bytes 4587520 | tf_op jit(solution)/shard_map/dot_general | solution.py:129
  169.9 30.7 %reduce-scatter.2.cloned.1.call-done = f32[32,128]{1,0:T(8,128)} async-done(((f32[32,1024]{1,0:T(8,128)}), f32[32,128]{1,0:T(8,128)}) %reduce-scatter.2.cloned.1.call-update) | async-done | bytes 16400 | tf_op jit(solution)/shard_map/reduce_scatter | solution.py:130
  200.7 1.3 add_convert_fusion.1
  (46 shorter events, 2.0 us)
Async XLA Ops:
  6.5 44.8 %copy-start = (bf16[4096,128]{1,0:T(8,128)(2,1)S(1)}, bf16[4096,128]{1,0:T(8,128)(2,1)}, u32[]{:S(2)}) copy-start(bf16[4096,128]{1,0:T(8,128)(2,1)} %param.18) | copy-start | bytes 3145732
  6.5 159.6 %all-reduce.2.cloned.1.call-start = ((), (), s32[]{:S(2)}) async-start(), calls=%async_computation.1 | async-start | bytes 524288 | tf_op jit(solution)/shard_map/psum | solution.py:128
  58.4 36.1 %copy-start.1 = (bf16[4096,128]{1,0:T(8,128)(2,1)S(1)}, bf16[4096,128]{1,0:T(8,128)(2,1)}, u32[]{:S(2)}) copy-start(bf16[4096,128]{1,0:T(8,128)(2,1)} %param.19) | copy-start | bytes 3145732
  58.4 36.1 %copy-start.4 = (f32[4096]{0:T(1024)S(1)}, f32[4096]{0:T(1024)}, u32[]{:S(2)}) copy-start(f32[4096]{0:T(1024)} %param.17) | copy-start | bytes 49156
  58.5 37.0 %copy-start.2 = (bf16[4096,128]{1,0:T(8,128)(2,1)S(1)}, bf16[4096,128]{1,0:T(8,128)(2,1)}, u32[]{:S(2)}) copy-start(bf16[4096,128]{1,0:T(8,128)(2,1)} %param.20) | copy-start | bytes 3145732
  75.0 0.6 copy-start.3
  97.3 1.4 collective-permute-start
  98.7 5.6 %collective-permute-start.1 = (f32[32,1024]{1,0:T(8,128)S(1)}, f32[32,1024]{1,0:T(8,128)S(1)}, u32[]{:S(2)}, u32[]{:S(2)}) collective-permute-start(f32[32,1024]{1,0:T(8,128)S(1)} %add.148), channel_id=1, source_target_pairs={{0,2},{1,3},{2,0},{3,1},{4,6},{5,7},{6,4},{7,5},{8,10},{9,11},{10,... | collective-permute-start | bytes 393224 | tf_op jit(solution)/shard_map/ppermute | solution.py:111
  104.3 8.5 %collective-permute-start.2 = (f32[32,1024]{1,0:T(8,128)S(1)}, f32[32,1024]{1,0:T(8,128)S(1)}, u32[]{:S(2)}, u32[]{:S(2)}) collective-permute-start(f32[32,1024]{1,0:T(8,128)S(1)} %add.149), channel_id=1, source_target_pairs={{0,4},{1,5},{2,6},{3,7},{4,0},{5,1},{6,2},{7,3},{8,12},{9,13},{10,... | collective-permute-start | bytes 393224 | tf_op jit(solution)/shard_map/ppermute | solution.py:111
  125.7 74.9 %reduce-scatter.2.cloned.1.call-start = ((), (), s32[]{:S(2)}) async-start(), calls=%async_computation.2 | async-start | bytes 147456 | tf_op jit(solution)/shard_map/reduce_scatter | solution.py:130
Sparse Core Ops, SparseCore 0:
  125.8 40.2 all-reduce.1
  170.1 30.5 reduce-scatter.1
